TPU v7x, 32 devices: a whole 2x2x4 slice. The times are simulated.
32 devices in a mesh: sp: 8 (over z, x), tp: 4 (over y, core).
Axes of the slice: x: 2, y: 2, z: 4, core: 2. Of those that a mesh axis runs over, the one named last changes fastest.
Arguments:
- residual_layer_input: bfloat16 [2048, 2048], P(('sp', 'tp')), may hold values from -6 to 6
- value_projected: bfloat16 [2048, 4096], P('sp', 'tp'), may hold values from -6 to 6
- key_projected: bfloat16 [2048, 2048], P('sp', 'tp'), may hold values from -6 to 6
- query_projected: bfloat16 [2048, 2048], P('sp', 'tp'), may hold values from -6 to 6
- output_gate_projected: bfloat16 [2048, 4096], P('sp', 'tp'), may hold values from -6 to 6
- step_projected_raw: bfloat16 [2, 2048, 64], P(None, 'sp', 'tp'), may hold values from -5.5 to 5
- head_decay_logarithm: float32 [2, 64], P(None, 'tp'), may hold values from -15 to -2.9
- position_extra_decay: float32 [2048, 64], P('sp', 'tp'), may hold values from -2.1 to 0
- value_filter_weight: bfloat16 [5, 4096], P(None, 'tp'), may hold values from -2.5 to 2.5
- key_filter_weight: bfloat16 [5, 2048], P(None, 'tp'), may hold values from -2.5 to 2.5
- query_filter_weight: bfloat16 [5, 2048], P(None, 'tp'), may hold values from -2.5 to 2.5
- head_norm_gain: float32 [4096], P('tp'), may hold values from 0.1 to 1.9
- mixer_output_matrix: bfloat16 [4096, 2048], P(None, 'tp'), may hold values from -0.09375 to 0.09375
- expert_norm_gain: float32 [2048], replicated, may hold values from 0.1 to 1.9
- routes: int32 [2048, 2], P('sp'), may hold values from 0 to 7, all different within a row; in each aligned block of 64 rows (0 to 63, 64 to 127, ...) at most 32 rows name the same one
- chosen_expert_weight: float32 [2048, 2], P(('sp', 'tp')), may hold values from 0.1 to 1
- expert_gate_matrix: bfloat16 [8, 2048, 4096], P('sp', None, 'tp'), may hold values from -0.125 to 0.125
- expert_up_matrix: bfloat16 [8, 2048, 4096], P('sp', None, 'tp'), may hold values from -0.125 to 0.125
- expert_down_matrix: bfloat16 [8, 4096, 2048], P('sp', 'tp'), may hold values from -0.09375 to 0.09375
Outputs:
- layer_output: bfloat16 [2048, 2048], P(('sp', 'tp'))
Inputs may be any that keep to these rules, and one draw needn't show every extreme that they name: `routes`: each row names 2 different experts; the rows of one device (aligned blocks of 64 rows) name one expert 32 times at most, and that most is reached.
All inputs are finite; a program needn't handle non-finite values.
Results may differ from a plain program's by a relative error of at most 0.015.
Values may be sent and summed in bfloat16 or wider, within the bound.
No kernel may reach another device: no remote copies, remote signals or barrier semaphores. Data moves between devices by JAX's collectives and lax.ppermute only.
A program may use at most 64 MiB of HBM per device.

v0:
```python
import jax
import jax.numpy as jnp
from jax import lax
from jax.sharding import PartitionSpec as P

HEAD_DIM = 64
STATE = 128
BLOCK = 128
TAPS = 5


epsilon = 1e-06
highest = lax.Precision.HIGHEST


def padded_2(cells, sides, width):
    for axis, dim in sides:
        count = lax.axis_size(axis)
        ends = count - 1
        head = lax.slice_in_dim(cells, 0, width, axis=dim)
        tail = lax.slice_in_dim(cells, cells.shape[dim] - width, cells.shape[dim], axis=dim)
        cells = jnp.concatenate(
            [
                lax.ppermute(tail, axis, [(i, (i + 1) % count) for i in range(ends)]),
                cells,
                lax.ppermute(head, axis, [((i + 1) % count, i) for i in range(ends)]),
            ],
            axis=dim,
        )
    return cells


def carried_in(x, axis, combine, identity, reverse):
    count, here = (lax.axis_size(axis), lax.axis_index(axis))
    everything = jax.tree.map(
        lambda part, kind: lax.all_gather(part.astype(kind), axis), x, (jnp.bfloat16, jnp.bfloat16)
    )
    start = jax.tree.map(
        lambda part, zero: jnp.broadcast_to(jnp.asarray(zero, part.dtype), part.shape), x, identity
    )

    def step(k, before):
        at = count - 1 - k if reverse else k
        reached = at > here if reverse else at < here
        new = combine(
            before, jax.tree.map(lambda part, own: part[at].astype(own.dtype), everything, x)
        )
        return jax.tree.map(lambda a, b: jnp.where(reached, a, b), new, before)

    return lax.fori_loop(0, count, step, start)


def prefix_matrix(length):
    row_index = lax.broadcasted_iota(jnp.int32, (length, length), 0)
    column_index = lax.broadcasted_iota(jnp.int32, (length, length), 1)
    return (column_index <= row_index).astype(jnp.float32)


def carry_combine(first_part, second_part):
    return (
        first_part[0] + second_part[0],
        jnp.exp(second_part[0])[..., None, None] * first_part[1] + second_part[1],
    )


def local_chain(states, totals, reverse):

    def advance(carried, operands):
        block_state, block_total = operands
        return (jnp.exp(block_total)[..., None, None] * carried + block_state, carried)

    start_state = jnp.zeros(states.shape[1:], jnp.float32)
    return lax.scan(advance, start_state, (states, totals), reverse=reverse)


def mix_tokens(
    value_projected,
    key_projected,
    query_projected,
    output_gate_projected,
    step_projected_raw,
    head_decay_logarithm,
    position_extra_decay,
    value_filter_weight,
    key_filter_weight,
    query_filter_weight,
    head_norm_gain,
):
    tokens = value_projected.shape[0]
    value_width = value_projected.shape[1]
    key_width = key_projected.shape[1]
    head_count = step_projected_raw.shape[2]
    group_count = key_width // STATE
    per_group = head_count // group_count
    blocks = tokens // BLOCK
    joined = jnp.concatenate([value_projected, key_projected, query_projected], axis=1)
    padded = padded_2(joined, (("sp", 0),), (TAPS - 1) // 2).astype(jnp.float32)
    weights = jnp.concatenate(
        [value_filter_weight, key_filter_weight, query_filter_weight], axis=1
    ).astype(jnp.float32)
    filtered = weights[0] * padded[0:tokens]
    for offset in range(1, TAPS):
        filtered = filtered + weights[offset] * padded[offset : offset + tokens]
    values = filtered[:, :value_width].astype(jnp.bfloat16)
    key_rows = jax.nn.silu(filtered[:, value_width : value_width + key_width]).astype(jnp.bfloat16)
    key_rows = key_rows.reshape(blocks, BLOCK, group_count, STATE)
    query_rows = jax.nn.silu(filtered[:, value_width + key_width :]).astype(jnp.bfloat16)
    query_rows = query_rows.reshape(blocks, BLOCK, group_count, STATE)
    positive_step_sizes = jax.nn.softplus(step_projected_raw.astype(jnp.float32))
    decay_logarithm = (
        -jnp.exp(head_decay_logarithm)[:, None, :] * positive_step_sizes
        + position_extra_decay[None]
    )
    scaled = (
        values.astype(jnp.float32).reshape(tokens, head_count, HEAD_DIM)[None]
        * positive_step_sizes[..., None]
    ).astype(jnp.bfloat16)
    scaled = scaled.reshape(2, blocks, BLOCK, group_count, per_group, HEAD_DIM)
    log_blocks = decay_logarithm.reshape(2, blocks, BLOCK, group_count, per_group)
    running = jnp.einsum("ls,dbsgh->dblgh", prefix_matrix(BLOCK), log_blocks, precision=highest)
    forward_cum = running[0]
    backward_excl = running[1] - log_blocks[1]
    forward_total = running[0][:, -1]
    backward_total = running[1][:, -1]
    scores = jnp.einsum("blgn,bsgn->blsg", query_rows, key_rows, preferred_element_type=jnp.float32)
    position = lax.broadcasted_iota(jnp.int32, (BLOCK,), 0)
    lower_mask = (position[None, :] <= position[:, None])[None, :, :, None, None]
    upper_mask = (position[None, :] >= position[:, None])[None, :, :, None, None]
    forward_gap = jnp.where(lower_mask, forward_cum[:, :, None] - forward_cum[:, None, :], -jnp.inf)
    backward_gap = jnp.where(
        upper_mask, backward_excl[:, None, :] - backward_excl[:, :, None], -jnp.inf
    )
    forward_weight = (scores[..., None] * jnp.exp(forward_gap)).astype(jnp.bfloat16)
    backward_weight = (scores[..., None] * jnp.exp(backward_gap)).astype(jnp.bfloat16)
    inner = jnp.einsum(
        "blsgh,bsghp->blghp", forward_weight, scaled[0], preferred_element_type=jnp.float32
    )
    inner = inner + jnp.einsum(
        "blsgh,bsghp->blghp", backward_weight, scaled[1], preferred_element_type=jnp.float32
    )
    key_wide = key_rows.astype(jnp.float32)[:, :, :, None, :]
    forward_keys = (jnp.exp(forward_total[:, None] - forward_cum)[..., None] * key_wide).astype(
        jnp.bfloat16
    )
    backward_keys = (jnp.exp(backward_excl)[..., None] * key_wide).astype(jnp.bfloat16)
    forward_state = jnp.einsum(
        "bsghn,bsghp->bghpn", forward_keys, scaled[0], preferred_element_type=jnp.float32
    )
    backward_state = jnp.einsum(
        "bsghn,bsghp->bghpn", backward_keys, scaled[1], preferred_element_type=jnp.float32
    )
    forward_final, forward_before = local_chain(forward_state, forward_total, False)
    backward_final, backward_before = local_chain(backward_state, backward_total, True)
    forward_sum = jnp.sum(forward_total, axis=0)
    backward_sum = jnp.sum(backward_total, axis=0)
    zero_total = jnp.zeros(forward_sum.shape, jnp.float32)
    zero_state = jnp.zeros(forward_final.shape, jnp.float32)
    entering = carried_in(
        (forward_sum, forward_final), "sp", carry_combine, (zero_total, zero_state), False
    )[1]
    leaving = carried_in(
        (backward_sum, backward_final), "sp", carry_combine, (zero_total, zero_state), True
    )[1]
    forward_prior = jnp.cumsum(forward_total, axis=0) - forward_total
    backward_after = backward_sum[None] - jnp.cumsum(backward_total, axis=0)
    forward_in = jnp.exp(forward_prior)[..., None, None] * entering[None] + forward_before
    backward_in = jnp.exp(backward_after)[..., None, None] * leaving[None] + backward_before
    forward_read = jnp.exp(forward_cum)[..., None] * jnp.einsum(
        "blgn,bghpn->blghp",
        query_rows,
        forward_in.astype(jnp.bfloat16),
        preferred_element_type=jnp.float32,
    )
    backward_read = jnp.exp(backward_total[:, None] - backward_excl)[..., None] * jnp.einsum(
        "blgn,bghpn->blghp",
        query_rows,
        backward_in.astype(jnp.bfloat16),
        preferred_element_type=jnp.float32,
    )
    mixer_raw = (inner + forward_read + backward_read).reshape(tokens, head_count, HEAD_DIM)
    gated = mixer_raw * jax.nn.silu(output_gate_projected.astype(jnp.float32)).reshape(
        tokens, head_count, HEAD_DIM
    )
    inverse_rms = lax.rsqrt(jnp.mean(gated * gated, axis=-1, keepdims=True) + epsilon)
    head_normed = (gated * inverse_rms * head_norm_gain.reshape(head_count, HEAD_DIM)).astype(
        jnp.bfloat16
    )
    return head_normed.reshape(tokens, head_count * HEAD_DIM)


def slot_table(route_rows, experts, capacity):
    flat_ids = route_rows.reshape(-1)
    expert_ids = lax.broadcasted_iota(jnp.int32, (flat_ids.shape[0], experts), 1)
    matches = (flat_ids[:, None] == expert_ids).astype(jnp.int32)
    earlier = jnp.cumsum(matches, axis=0) - matches
    rank_in = jnp.sum(matches * earlier, axis=1)
    return (flat_ids * capacity + rank_in).reshape(route_rows.shape)


def dispatch_rows(slots, token_rows, places):
    place_ids = lax.broadcasted_iota(jnp.int32, (places,) + slots.shape, 0)
    one_hot = jnp.sum((place_ids == slots[None]).astype(jnp.float32), axis=2).astype(jnp.bfloat16)
    return jnp.dot(one_hot, token_rows, preferred_element_type=jnp.float32).astype(jnp.bfloat16)


def shards(
    residual_layer_input,
    value_projected,
    key_projected,
    query_projected,
    output_gate_projected,
    step_projected_raw,
    head_decay_logarithm,
    position_extra_decay,
    value_filter_weight,
    key_filter_weight,
    query_filter_weight,
    head_norm_gain,
    mixer_output_matrix,
    expert_norm_gain,
    routes,
    chosen_expert_weight,
    expert_gate_matrix,
    expert_up_matrix,
    expert_down_matrix,
):
    heads_out = mix_tokens(
        value_projected,
        key_projected,
        query_projected,
        output_gate_projected,
        step_projected_raw,
        head_decay_logarithm,
        position_extra_decay,
        value_filter_weight,
        key_filter_weight,
        query_filter_weight,
        head_norm_gain,
    )
    projected = jnp.dot(
        lax.all_gather(heads_out, "tp", axis=1, tiled=True),
        mixer_output_matrix,
        preferred_element_type=jnp.float32,
    ).astype(jnp.bfloat16)
    mixer_out = lax.all_to_all(projected, "tp", split_axis=0, concat_axis=1, tiled=True)
    middle = (residual_layer_input.astype(jnp.float32) + mixer_out.astype(jnp.float32)).astype(
        jnp.bfloat16
    )
    residual = middle.astype(jnp.float32)
    normed = (
        residual
        * lax.rsqrt(jnp.mean(residual * residual, axis=-1, keepdims=True) + epsilon)
        * expert_norm_gain
    ).astype(jnp.bfloat16)
    own_rows = normed.shape[0]
    model_width = normed.shape[1]
    top_count = routes.shape[1]
    experts = lax.axis_size("sp")
    capacity = 2 * own_rows * top_count // experts
    places = experts * capacity
    position = lax.axis_index("tp")
    own_routes = lax.dynamic_slice_in_dim(routes, position * own_rows, own_rows, 0)
    own_slots = slot_table(own_routes, experts, capacity)
    outgoing = dispatch_rows(own_slots, normed, places)
    received = lax.all_to_all(
        outgoing.reshape(experts, capacity, model_width),
        "sp",
        split_axis=0,
        concat_axis=0,
        tiled=True,
    )
    arrived = lax.all_gather(received[None], "tp", axis=0, tiled=True)
    slot_rows = arrived.reshape(-1, model_width)
    gate_value = jnp.dot(slot_rows, expert_gate_matrix[0], preferred_element_type=jnp.float32)
    up_value = jnp.dot(slot_rows, expert_up_matrix[0], preferred_element_type=jnp.float32)
    hidden = (jax.nn.silu(gate_value) * up_value).astype(jnp.bfloat16)
    partial_sum = jnp.dot(hidden, expert_down_matrix[0], preferred_element_type=jnp.float32).astype(
        jnp.bfloat16
    )
    summed = lax.psum_scatter(
        partial_sum.astype(jnp.float32).reshape(arrived.shape).astype(jnp.bfloat16),
        "tp",
        scatter_dimension=0,
        tiled=True,
    )
    results = summed.reshape(experts, capacity, model_width)
    returned = lax.all_to_all(results, "sp", split_axis=0, concat_axis=0, tiled=True)
    chosen = (
        lax.broadcasted_iota(jnp.int32, (own_rows, top_count, places), 2) == own_slots[:, :, None]
    )
    mixing = jnp.sum(jnp.where(chosen, chosen_expert_weight[:, :, None], 0.0), axis=1)
    expert_mix = jnp.dot(
        mixing, returned.reshape(places, model_width).astype(jnp.float32), precision=highest
    )
    return (residual + expert_mix).astype(jnp.bfloat16)


def solution(mesh):
    return jax.shard_map(
        shards,
        mesh=mesh,
        in_specs=(
            P(("sp", "tp"), None),
            P("sp", "tp"),
            P("sp", "tp"),
            P("sp", "tp"),
            P("sp", "tp"),
            P(None, "sp", "tp"),
            P(None, "tp"),
            P("sp", "tp"),
            P(None, "tp"),
            P(None, "tp"),
            P(None, "tp"),
            P("tp"),
            P(None, "tp"),
            P(),
            P("sp", None),
            P(("sp", "tp"), None),
            P("sp", None, "tp"),
            P("sp", None, "tp"),
            P("sp", "tp", None),
        ),
        out_specs=P(("sp", "tp"), None),
        check_vma=False,
    )
```

profile of v0, /device:TPU:0, one launch (start us, length us, event | category | flops | bytes accessed | tf_op | source)
XLA Modules:
  0.0 367.2 jit_solution(2573154776203931177)
XLA Ops:
  11.2 4.9 %collective-permute-start = (bf16[2,2048]{0,1:T(8,128)(2,1)}, bf16[2,2048]{0,1:T(8,128)(2,1)S(1)}, u32[]{:S(2)}, u32[]{:S(2)}) collective-permute-start(bf16[2,2048]{0,1:T(8,128)(2,1)} %get-tuple-element.493), channel_id=1, source_target_pairs={{0,4},{4,8},{8,12},{12,16},{16,20},{20,24},{24,28},{1,5},{5,9},{9,... | collective-permute-start | bytes 24584 | tf_op jit(solution)/shard_map/ppermute | solution.py:24
  16.1 1.3 collective-permute-start.1
  18.1 20.6 %collective-permute-done = bf16[2,2048]{0,1:T(8,128)(2,1)S(1)} collective-permute-done((bf16[2,2048]{0,1:T(8,128)(2,1)}, bf16[2,2048]{0,1:T(8,128)(2,1)S(1)}, u32[]{:S(2)}, u32[]{:S(2)}) %collective-permute-start) | collective-permute-done | bytes 8224 | tf_op jit(solution)/shard_map/ppermute | solution.py:24
  39.6 3.9 %fusion.14 = f32[256,2048]{0,1:T(8,128)S(1)} fusion(f32[260,2048]{0,1:T(8,128)S(1)} %maximum_convert_fusion, f32[2048]{0:T(1024)S(1)} %bitcast.182, f32[2048]{0:T(1024)S(1)} %bitcast.179, f32[2048]{0:T(1024)S(1)} %bitcast.180, f32[2048]{0:T(1024)S(1)} %bitcast.181, f32[2048]{0:T(1024)S(1)} %bitcast.178), kind=kLoop, calls=%fused_computation.24 | loop fusion | flops 4718592 | bytes 12623872 | tf_op jit(solution)/shard_map/add | solution.py:103
  49.3 1.2 copy.113
  50.6 1.3 convert_multiply_fusion
  51.8 2.7 reshape.265
  54.6 20.9 %all-gather.5 = bf16[8,4,4]{2,1,0:T(4,128)(2,1)S(1)} all-gather(bf16[1,4,4]{2,1,0:T(4,128)(2,1)S(1)} %bitcast.183), channel_id=2, replica_groups=mesh['sp'=8,'tp'=4] {'sp'}, dimensions={0}, use_global_device_ids=true | all-gather | bytes 288 | tf_op jit(solution)/shard_map/all_gather | solution.py:36
  75.5 16.6 %all-gather.6 = bf16[8,4,4]{2,1,0:T(4,128)(2,1)S(1)} all-gather(bf16[1,4,4]{2,1,0:T(4,128)(2,1)S(1)} %convert_bitcast_fusion.1), channel_id=4, replica_groups=mesh['sp'=8,'tp'=4] {'sp'}, dimensions={0}, use_global_device_ids=true | all-gather | bytes 288 | tf_op jit(solution)/shard_map/all_gather | solution.py:36
  92.2 1.7 reshape.262
  93.9 2.0 squeeze.64
  95.8 2.1 fusion.30
  99.1 2.0 while.62
  104.7 2.0 fusion.28
  106.7 1.9 fusion.22
  108.6 9.1 %while.61 = (s32[]{:T(128)}, f32[4,4,64,128]{3,2,1,0:T(8,128)S(1)}, s32[]{:T(128)}, bf16[8,4,4]{2,1,0:T(4,128)(2,1)S(1)}, bf16[8,4,4,64,128]{4,3,2,1,0:T(8,128)(2,1)}, /*index=5*/s32[]{:T(128)}, s32[]{:T(128)}) while((s32[]{:T(128)}, f32[4,4,64,128]{3,2,1,0:T(8,128)S(1)}, s32[]{:T(128)}, bf16[8,4,4]{2,1,0:T(4,128)(2,1)S(1)}, ...), condition=%wide.region_5.6_spmd.clone, body=%wide.region_4.5_spmd.clone.sunk | while | flops 655380 | bytes 1310985 | solution.py:50
  117.7 32.7 %all-gather.16.cloned.1.call-done = bf16[32,4,64,128]{3,2,1,0:T(8,128)(2,1)} async-done(((bf16[4,4,64,128]{3,2,1,0:T(8,128)(2,1)}), bf16[32,4,64,128]{3,2,1,0:T(8,128)(2,1)}) %all-gather.16.cloned.1.call-update) | async-done | bytes 2097168 | tf_op jit(solution)/shard_map/all_gather | solution.py:36
  150.4 9.2 %while.63 = (s32[]{:T(128)}, f32[4,4,64,128]{3,2,1,0:T(8,128)S(1)}, s32[]{:T(128)}, bf16[8,4,4]{2,1,0:T(4,128)(2,1)S(1)}, bf16[8,4,4,64,128]{4,3,2,1,0:T(8,128)(...) while((s32[]{:T(128)}, f32[4,4,64,128]{3,2,1,0:T(8,128)S(1)}, s32[]{:T(128)}, ...), condition=%wide.region_11.12_spmd.clone, body=%wide.region_10.11_spmd.clone.sunk | while | flops 655384 | bytes 1311047 | solution.py:50
  159.7 1.7 fusion.21
  165.1 20.3 %all-gather.12.cloned.1.call-done = bf16[256,4096]{0,1:T(8,128)(2,1)} async-done(((bf16[256,1024]{0,1:T(8,128)(2,1)}), bf16[256,4096]{0,1:T(8,128)(2,1)}) %all-gather.12.cloned.1.call-update) | async-done | bytes 2097168 | tf_op jit(solution)/shard_map/all_gather | solution.py:241
  185.3 4.8 %convolution_convert_fusion.1 = bf16[256,512]{1,0:T(8,128)(2,1)} fusion(bf16[256,4096]{0,1:T(8,128)(2,1)} %all-gather.12.cloned.1.call-done, bf16[4096,512]{1,0:T(8,128)(2,1)} %param.39), kind=kOutput, calls=%fused_computation.49 | convolution fusion | flops 1073872896 | bytes 6553600 | tf_op jit(solution)/shard_map/dot_general | solution.py:240
  190.1 3.5 all-to-all-start
  193.9 5.7 %all-to-all-done = bf16[4,64,512]{2,1,0:T(8,128)(2,1)S(1)} async-done(((bf16[4,64,512]{2,1,0:T(8,128)(2,1)}), bf16[4,64,512]{2,1,0:T(8,128)(2,1)S(1)}, u32[]{:S(2)}, u32[]{:S(2)}) %all-to-all-start) | async-done | bytes 262176 | tf_op jit(solution)/shard_map/all_to_all | solution.py:245
  200.5 30.9 %all_to_all.23 = bf16[8,32,2048]{2,1,0:T(8,128)(2,1)} all-to-all(bf16[8,32,2048]{2,1,0:T(8,128)(2,1)S(1)} %bitcast.169), channel_id=1, replica_groups=mesh['sp'=8,'tp'=4] {'sp'}, dimensions={0} | all-to-all | bytes 2097152 | tf_op jit(solution)/shard_map/all_to_all | solution.py:265
  231.5 32.8 %all-gather.18.cloned.1.call-done = bf16[32,32,2048]{2,1,0:T(8,128)(2,1)} async-done(((bf16[8,32,2048]{2,1,0:T(8,128)(2,1)}), bf16[32,32,2048]{2,1,0:T(8,128)(2,1)}) %all-gather.18.cloned.1.call-update) | async-done | bytes 4194320 | tf_op jit(solution)/shard_map/all_gather | solution.py:272
  264.3 7.6 %fusion.4 = f32[1024,1024]{1,0:T(8,128)S(1)} fusion(bf16[1024,2048]{1,0:T(8,128)(2,1)} %bitcast.184, bf16[1,2048,1024]{2,1,0:T(8,128)(2,1)} %param.44), kind=kOutput, calls=%fused_computation.14 | convolution fusion | flops 4294967296 | bytes 12582912 | tf_op jit(solution)/shard_map/dot_general | solution.py:275
  272.0 5.4 %multiply_convert_fusion = bf16[1024,1024]{1,0:T(8,128)(2,1)S(1)} fusion(f32[1024,1024]{1,0:T(8,128)S(1)} %fusion.4, bf16[1024,2048]{1,0:T(8,128)(2,1)S(1)} %bitcast.185, bf16[1,2048,1024]{2,1,0:T(8,128)(2,1)S(1)} %copy-done.21), kind=kOutput, calls=%fused_computation.18 | convolution fusion | flops 4301258752 | bytes 14680064 | tf_op jit(solution)/shard_map/dot_general | solution.py:274
  277.4 6.1 %fusion.8 = bf16[1024,2048]{1,0:T(8,128)(2,1)} fusion(bf16[1024,1024]{1,0:T(8,128)(2,1)S(1)} %multiply_convert_fusion, bf16[1,1024,2048]{2,1,0:T(8,128)(2,1)S(1)} %copy-done.22), kind=kOutput, calls=%fused_computation.19 | convolution fusion | flops 4297064448 | bytes 10485760 | tf_op jit(solution)/shard_map/dot_general | solution.py:277
  283.5 44.7 %reduce-scatter.2.cloned.1.call-done = bf16[1,8,32,2048]{3,2,1,0:T(8,128)(2,1)} async-done(((bf16[4,8,32,2048]{3,2,1,0:T(8,128)(2,1)}), bf16[1,8,32,2048]{3,2,1,0:T(8,128)(2,1)}) %reduce-scatter.2.cloned.1.call-update) | async-done | bytes 1048592 | tf_op jit(solution)/shard_map/reduce_scatter | solution.py:280
  328.2 5.5 %all-to-all-start.2 = ((bf16[8,32,2048]{2,1,0:T(8,128)(2,1)}), bf16[8,32,2048]{2,1,0:T(8,128)(2,1)S(1)}, u32[]{:S(2)}, u32[]{:S(2)}) async-start(bf16[8,32,2048]{2,1,0:T(8,128)(2,1)} %bitcast.173), calls=%async_computation.3 | async-start | bytes 2097152 | tf_op jit(solution)/shard_map/all_to_all | solution.py:287
  333.8 25.6 %all-to-all-done.2 = bf16[8,32,2048]{2,1,0:T(8,128)(2,1)S(1)} async-done(((bf16[8,32,2048]{2,1,0:T(8,128)(2,1)}), bf16[8,32,2048]{2,1,0:T(8,128)(2,1)S(1)}, u32[]{:S(2)}, u32[]{:S(2)}) %all-to-all-start.2) | async-done | bytes 1048608 | tf_op jit(solution)/shard_map/all_to_all | solution.py:287
  359.4 1.4 fusion.13
  (169 shorter events, 41.3 us)
Async XLA Ops:
  6.5 102.1 %all-gather.14.cloned.1.call-start = ((), (), s32[]{:S(2)}) async-start(), calls=%async_computation.6 | async-start | bytes 2359296 | tf_op jit(solution)/shard_map/all_gather | solution.py:36
  10.0 7.4 %copy-start.20 = (f32[2,16]{1,0:T(2,128)S(1)}, f32[2,16]{1,0:T(2,128)}, u32[]{:S(2)}) copy-start(f32[2,16]{1,0:T(2,128)} %param.33) | copy-start | bytes 388
  10.0 7.4 %copy-start.11 = (bf16[2,256,16]{1,2,0:T(8,128)(2,1)S(1)}, bf16[2,256,16]{1,2,0:T(8,128)(2,1)}, u32[]{:S(2)}) copy-start(bf16[2,256,16]{1,2,0:T(8,128)(2,1)} %param.32) | copy-start | bytes 49156
  10.0 7.4 %copy-start.12 = (f32[256,16]{0,1:T(8,128)S(1)}, f32[256,16]{0,1:T(8,128)}, u32[]{:S(2)}) copy-start(f32[256,16]{0,1:T(8,128)} %param.34) | copy-start | bytes 49156
  10.0 8.0 %copy-start.13 = (bf16[5,1024]{1,0:T(8,128)(2,1)S(1)}, bf16[5,1024]{1,0:T(8,128)(2,1)}, u32[]{:S(2)}) copy-start(bf16[5,1024]{1,0:T(8,128)(2,1)} %param.35) | copy-start | bytes 30724
  10.0 8.0 %copy-start.15 = (bf16[5,512]{1,0:T(8,128)(2,1)S(1)}, bf16[5,512]{1,0:T(8,128)(2,1)}, u32[]{:S(2)}) copy-start(bf16[5,512]{1,0:T(8,128)(2,1)} %param.37) | copy-start | bytes 15364
  10.0 8.0 %copy-start.16 = (bf16[5,512]{1,0:T(8,128)(2,1)S(1)}, bf16[5,512]{1,0:T(8,128)(2,1)}, u32[]{:S(2)}) copy-start(bf16[5,512]{1,0:T(8,128)(2,1)} %param.36) | copy-start | bytes 15364
  11.2 27.6 %collective-permute-start = (bf16[2,2048]{0,1:T(8,128)(2,1)}, bf16[2,2048]{0,1:T(8,128)(2,1)S(1)}, u32[]{:S(2)}, u32[]{:S(2)}) collective-permute-start(bf16[2,2048]{0,1:T(8,128)(2,1)} %get-tuple-element.493), channel_id=1, source_target_pairs={{0,4},{4,8},{8,12},{12,16},{16,20},{20,24},{24,28},{1,5},{5,9},{9,... | collective-permute-start | bytes 24584 | tf_op jit(solution)/shard_map/ppermute | solution.py:24
  16.1 22.7 %collective-permute-start.1 = (bf16[2,2048]{0,1:T(8,128)(2,1)S(1)}, bf16[2,2048]{0,1:T(8,128)(2,1)S(1)}, u32[]{:S(2)}, u32[]{:S(2)}) collective-permute-start(bf16[2,2048]{0,1:T(8,128)(2,1)S(1)} %get-tuple-element.494), channel_id=1, source_target_pairs={{4,0},{8,4},{12,8},{16,12},{20,16},{24,20},{28,24},{5,1},{9,5},{13... | collective-permute-start | bytes 24584 | tf_op jit(solution)/shard_map/ppermute | solution.py:26
  46.1 1.8 copy-start
  48.3 6.2 %copy-start.1 = (f32[2,4,4,64,128]{4,3,2,1,0:T(8,128)}, f32[2,4,4,64,128]{4,3,2,1,0:T(8,128)S(1)}, u32[]{:S(2)}) copy-start(f32[2,4,4,64,128]{4,3,2,1,0:T(8,128)S(1)} %get-tuple-element.365) | copy-start | bytes 3145732
  49.2 101.2 %all-gather.16.cloned.1.call-start = ((), (), s32[]{:S(2)}) async-start(), calls=%async_computation.7 | async-start | bytes 2359296 | tf_op jit(solution)/shard_map/all_gather | solution.py:36
  101.1 3.3 copy-start.5
  101.1 3.5 copy-start.7
  101.9 83.4 %all-gather.12.cloned.1.call-start = ((), (), s32[]{:S(2)}) async-start(), calls=%async_computation.4 | async-start | bytes 2621440 | tf_op jit(solution)/shard_map/all_gather | solution.py:241
  104.5 2.2 copy-start.8
  104.7 2.0 copy-start.9
  150.4 9.2 %copy-start.2 = (f32[2,4,4,64,128]{4,3,2,1,0:T(8,128)S(1)}, f32[2,4,4,64,128]{4,3,2,1,0:T(8,128)}, u32[]{:S(2)}) copy-start(f32[2,4,4,64,128]{4,3,2,1,0:T(8,128)} %copy-done.1) | copy-start | bytes 3145732
  159.7 1.8 copy-start.3
  159.7 1.8 copy-start.4
  162.0 0.9 copy-start.17
  162.0 2.1 copy-start.18
  190.1 9.6 %copy-start.10 = (bf16[64,2048]{1,0:T(8,128)(2,1)S(1)}, bf16[64,2048]{1,0:T(8,128)(2,1)}, u32[]{:S(2)}) copy-start(bf16[64,2048]{1,0:T(8,128)(2,1)} %param.27) | copy-start | bytes 786436
  190.1 9.8 %copy-start.14 = (f32[2048]{0:T(1024)S(1)}, f32[2048]{0:T(1024)}, u32[]{:S(2)}) copy-start(f32[2048]{0:T(1024)} %param.40) | copy-start | bytes 24580
  190.1 9.5 %all-to-all-start = ((bf16[4,64,512]{2,1,0:T(8,128)(2,1)}), bf16[4,64,512]{2,1,0:T(8,128)(2,1)S(1)}, u32[]{:S(2)}, u32[]{:S(2)}) async-start(bf16[4,64,512]{2,1,0:T(8,128)(2,1)} %bitcast.22), calls=%async_computation | async-start | bytes 524288 | tf_op jit(solution)/shard_map/all_to_all | solution.py:245
  193.7 70.6 %all-gather.18.cloned.1.call-start = ((), (), s32[]{:S(2)}) async-start(), calls=%async_computation.8 | async-start | bytes 5242880 | tf_op jit(solution)/shard_map/all_gather | solution.py:272
  231.4 96.7 %reduce-scatter.2.cloned.1.call-start = ((), (), s32[]{:S(2)}) async-start(), calls=%async_computation.5 | async-start | bytes 5242880 | tf_op jit(solution)/shard_map/reduce_scatter | solution.py:280
  264.3 7.7 %copy-start.21 = (bf16[1,2048,1024]{2,1,0:T(8,128)(2,1)S(1)}, bf16[1,2048,1024]{2,1,0:T(8,128)(2,1)}, u32[]{:S(2)}) copy-start(bf16[1,2048,1024]{2,1,0:T(8,128)(2,1)} %param.43) | copy-start | bytes 12582916
  264.3 7.7 %copy-start.23 = (bf16[32,32,2048]{2,1,0:T(8,128)(2,1)S(1)}, bf16[32,32,2048]{2,1,0:T(8,128)(2,1)}, u32[]{:S(2)}) copy-start(bf16[32,32,2048]{2,1,0:T(8,128)(2,1)} %all-gather.18.cloned.1.call-done) | copy-start | bytes 12582916
  272.0 5.4 %copy-start.22 = (bf16[1,1024,2048]{2,1,0:T(8,128)(2,1)S(1)}, bf16[1,1024,2048]{2,1,0:T(8,128)(2,1)}, u32[]{:S(2)}) copy-start(bf16[1,1024,2048]{2,1,0:T(8,128)(2,1)} %param.45) | copy-start | bytes 12582916
  283.4 50.2 %copy-start.19 = (f32[64,2]{0,1:T(2,128)S(1)}, f32[64,2]{0,1:T(2,128)}, u32[]{:S(2)}) copy-start(f32[64,2]{0,1:T(2,128)} %param.42) | copy-start | bytes 1540
  328.2 31.2 %all-to-all-start.2 = ((bf16[8,32,2048]{2,1,0:T(8,128)(2,1)}), bf16[8,32,2048]{2,1,0:T(8,128)(2,1)S(1)}, u32[]{:S(2)}, u32[]{:S(2)}) async-start(bf16[8,32,2048]{2,1,0:T(8,128)(2,1)} %bitcast.173), calls=%async_computation.3 | async-start | bytes 2097152 | tf_op jit(solution)/shard_map/all_to_all | solution.py:287
  (1 other events, 0.8 us)
Sparse Core Ops, SparseCore 0:
  49.3 51.2 all-gather.13
  102.7 47.6 all-gather.15
  164.2 21.0 all-gather.11
  231.5 32.7 all-gather.17
  283.6 44.5 reduce-scatter.1
where the time goes:
time: 368 us; the launch traced here: 367 us
  waiting for transfers between devices  183 us (50%)
  blocking collectives  68.4 us (19%)
  matrix products  36.4 us (10%)
  other arithmetic  31.6 us (9%)
  local copies, waits for them, and re-layouts  18.2 us (5%)
  starting transfers between devices  15.6 us (4%)
  between operations  13.9 us (4%)
    reduce_scatter x1, waiting for transfers between devices, shards(): lax.psum_scatter(partial_sum.astype(jnp.float32).reshape(arrived.shape).a...  44.7 us
    all_gather x2, blocking collectives, carried_in(): lax.all_gather(part.astype(kind), axis)  37.5 us
    all_gather x1, waiting for transfers between devices, shards(): arrived = lax.all_gather(received[None], 'tp', axis=0, tiled=True)  32.8 us
    all_gather x2, waiting for transfers between devices, carried_in(): lax.all_gather(part.astype(kind), axis)  32.7 us
    all_to_all x1, blocking collectives, shards(): lax.all_to_all(outgoing.reshape(experts, capacity, model_width), 'sp', sp...  30.9 us
    all_to_all x1, waiting for transfers between devices, shards(): lax.all_to_all(results, 'sp', split_axis=0, concat_axis=0, tiled=True)  25.6 us
    ppermute x1, waiting for transfers between devices, padded_2(): lax.ppermute(tail, axis, [(i, (i + 1) % count) for i in range(ends)])  20.6 us
    all_gather x1, waiting for transfers between devices, shards(): lax.all_gather(heads_out, 'tp', axis=1, tiled=True)  20.3 us
  transfers between devices with their start and end apart: 9, of which 7 were waited for; matrix products, arithmetic and copies ran while one was open for 9% of the time, Pallas kernels for 0%

commit v1 on v0

--- a/solution.py
+++ b/solution.py
@@ -30,37 +30,43 @@
     return cells
 
 
-def carried_in(x, axis, combine, identity, reverse):
-    count, here = (lax.axis_size(axis), lax.axis_index(axis))
-    everything = jax.tree.map(
-        lambda part, kind: lax.all_gather(part.astype(kind), axis), x, (jnp.bfloat16, jnp.bfloat16)
-    )
-    start = jax.tree.map(
-        lambda part, zero: jnp.broadcast_to(jnp.asarray(zero, part.dtype), part.shape), x, identity
-    )
-
-    def step(k, before):
-        at = count - 1 - k if reverse else k
-        reached = at > here if reverse else at < here
-        new = combine(
-            before, jax.tree.map(lambda part, own: part[at].astype(own.dtype), everything, x)
-        )
-        return jax.tree.map(lambda a, b: jnp.where(reached, a, b), new, before)
-
-    return lax.fori_loop(0, count, step, start)
+def carried_states(totals, states):
+    count = lax.axis_size("sp")
+    heads = totals.shape[1]
+    _, depth, columns = states.shape
+    decay = jnp.exp(totals).reshape(1, 2 * heads)
+    high = decay.astype(jnp.bfloat16)
+    low = (decay - high.astype(jnp.float32)).astype(jnp.bfloat16)
+    extra = jnp.broadcast_to(jnp.concatenate([high, low], axis=1), (depth, 4 * heads))
+    sent = jnp.concatenate(
+        [states[0].astype(jnp.bfloat16), states[1].astype(jnp.bfloat16), extra], axis=1
+    )
+    sent = sent.reshape(count, depth // count, sent.shape[1])
+    arrived = lax.all_to_all(sent, "sp", split_axis=0, concat_axis=0, tiled=True)
+    rows = arrived.astype(jnp.float32)
+    tail = rows[:, 0, 2 * columns :]
+    decays = jnp.repeat(tail[:, : 2 * heads] + tail[:, 2 * heads :], columns // heads, axis=1)
+    entering = [jnp.zeros((depth // count, columns), jnp.float32)]
+    leaving = [jnp.zeros((depth // count, columns), jnp.float32)]
+    for k in range(count - 1):
+        entering.append(entering[-1] * decays[k, :columns] + rows[k, :, :columns])
+        back = count - 1 - k
+        leaving.append(leaving[-1] * decays[back, columns:] + rows[back, :, columns : 2 * columns])
+    answer = jnp.stack(
+        [
+            jnp.concatenate([a, b], axis=1)
+            for a, b in zip(entering, leaving[::-1])
+        ]
+    ).astype(jnp.bfloat16)
+    back = lax.all_to_all(answer, "sp", split_axis=0, concat_axis=0, tiled=True)
+    back = back.reshape(depth, 2 * columns).astype(jnp.float32)
+    return back[:, :columns], back[:, columns:]
 
 
 def prefix_matrix(length):
     row_index = lax.broadcasted_iota(jnp.int32, (length, length), 0)
     column_index = lax.broadcasted_iota(jnp.int32, (length, length), 1)
     return (column_index <= row_index).astype(jnp.float32)
-
-
-def carry_combine(first_part, second_part):
-    return (
-        first_part[0] + second_part[0],
-        jnp.exp(second_part[0])[..., None, None] * first_part[1] + second_part[1],
-    )
 
 
 def local_chain(states, totals, reverse):
@@ -153,14 +159,13 @@
     backward_final, backward_before = local_chain(backward_state, backward_total, True)
     forward_sum = jnp.sum(forward_total, axis=0)
     backward_sum = jnp.sum(backward_total, axis=0)
-    zero_total = jnp.zeros(forward_sum.shape, jnp.float32)
-    zero_state = jnp.zeros(forward_final.shape, jnp.float32)
-    entering = carried_in(
-        (forward_sum, forward_final), "sp", carry_combine, (zero_total, zero_state), False
-    )[1]
-    leaving = carried_in(
-        (backward_sum, backward_final), "sp", carry_combine, (zero_total, zero_state), True
-    )[1]
+    to_columns = lambda x: x.reshape(-1, STATE).T
+    to_states = lambda x: x.T.reshape(forward_final.shape)
+    entering, leaving = carried_states(
+        jnp.stack([forward_sum.reshape(-1), backward_sum.reshape(-1)]),
+        jnp.stack([to_columns(forward_final), to_columns(backward_final)]),
+    )
+    entering, leaving = to_states(entering), to_states(leaving)
     forward_prior = jnp.cumsum(forward_total, axis=0) - forward_total
     backward_after = backward_sum[None] - jnp.cumsum(backward_total, axis=0)
     forward_in = jnp.exp(forward_prior)[..., None, None] * entering[None] + forward_before
@@ -188,19 +193,84 @@
     return head_normed.reshape(tokens, head_count * HEAD_DIM)
 
 
-def slot_table(route_rows, experts, capacity):
+def exchange(x, axis, distance):
+    count = lax.axis_size(axis)
+    return lax.ppermute(x, axis, [(i, i ^ distance) for i in range(count)])
+
+
+def bits_of(count):
+    return [1 << k for k in range(count.bit_length() - 1)]
+
+
+def gather_rows(rows, axis):
+    blocks = rows[None]
+    order = [0]
+    for bit in reversed(bits_of(lax.axis_size(axis))):
+        blocks = jnp.concatenate([blocks, exchange(blocks, axis, bit)], axis=0)
+        order = order + [b ^ bit for b in order]
+    return blocks, order
+
+
+def scatter_rows(blocks, axis):
+    for bit in bits_of(lax.axis_size(axis)):
+        half = blocks.shape[0] // 2
+        received = exchange(blocks[half:], axis, bit)
+        blocks = (blocks[:half].astype(jnp.float32) + received.astype(jnp.float32)).astype(
+            jnp.bfloat16
+        )
+    return blocks[0]
+
+
+def slot_table(route_rows, experts, capacity, here):
     flat_ids = route_rows.reshape(-1)
     expert_ids = lax.broadcasted_iota(jnp.int32, (flat_ids.shape[0], experts), 1)
-    matches = (flat_ids[:, None] == expert_ids).astype(jnp.int32)
-    earlier = jnp.cumsum(matches, axis=0) - matches
-    rank_in = jnp.sum(matches * earlier, axis=1)
-    return (flat_ids * capacity + rank_in).reshape(route_rows.shape)
-
-
-def dispatch_rows(slots, token_rows, places):
-    place_ids = lax.broadcasted_iota(jnp.int32, (places,) + slots.shape, 0)
-    one_hot = jnp.sum((place_ids == slots[None]).astype(jnp.float32), axis=2).astype(jnp.bfloat16)
-    return jnp.dot(one_hot, token_rows, preferred_element_type=jnp.float32).astype(jnp.bfloat16)
+    matches = (flat_ids[:, None] == expert_ids).astype(jnp.float32)
+    below = prefix_matrix(flat_ids.shape[0]).astype(jnp.bfloat16)
+    running = jnp.dot(
+        below, matches.astype(jnp.bfloat16), preferred_element_type=jnp.float32
+    )
+    rank_in = (jnp.sum(matches * running, axis=1) - 1.0).astype(jnp.int32)
+    return ((flat_ids ^ here) * capacity + rank_in).reshape(route_rows.shape)
+
+
+def reduce_columns(heads_out, own_columns, width):
+    axis = "tp"
+    count = lax.axis_size(axis)
+    me = lax.axis_index(axis)
+    blocks = [
+        jnp.dot(heads_out, part, preferred_element_type=jnp.float32).astype(jnp.bfloat16)
+        for part in own_columns
+    ]
+    rows = heads_out.shape[0] // count
+    partial = jnp.stack([b.reshape(count, rows, width) for b in blocks], axis=2)
+    for bit in bits_of(count):
+        half = partial.shape[0] // 2
+        pairs = partial.reshape(half, 2, rows, count, width)
+        mine = (me // bit) % 2
+        send = lax.dynamic_index_in_dim(pairs, 1 - mine, 1, keepdims=False)
+        keep = lax.dynamic_index_in_dim(pairs, mine, 1, keepdims=False)
+        received = exchange(send, axis, bit)
+        received = jnp.stack([received[:, :, c ^ bit] for c in range(count)], axis=2)
+        partial = (keep.astype(jnp.float32) + received.astype(jnp.float32)).astype(jnp.bfloat16)
+    final = partial[0]
+    for bit in bits_of(count):
+        swapped = jnp.stack([final[:, c ^ bit] for c in range(count)], axis=1)
+        final = jnp.where((me // bit) % 2 == 1, swapped, final)
+    return final.reshape(rows, count * width)
+
+
+def own_row_blocks(matrix, rows):
+    me = lax.axis_index("tp")
+    parts = []
+    for t in range(lax.axis_size("tp")):
+        block = lax.dynamic_slice_in_dim(matrix, (me ^ t) * rows, rows, 0)
+        parts.append(exchange(block, "tp", t) if t else block)
+    return parts
+
+
+def chunks_of(experts):
+    quarter = max(experts // 4, 1)
+    return [range(0, 2 * quarter), range(2 * quarter, 3 * quarter), range(3 * quarter, experts)]
 
 
 def shards(
@@ -224,6 +294,27 @@
     expert_up_matrix,
     expert_down_matrix,
 ):
+    experts = lax.axis_size("sp")
+    here = lax.axis_index("sp")
+    position = lax.axis_index("tp")
+    own_rows, model_width = residual_layer_input.shape
+    top_count = routes.shape[1]
+    capacity = 2 * own_rows * top_count // experts
+    places = experts * capacity
+    own_columns = own_row_blocks(mixer_output_matrix, value_projected.shape[1])
+    own_routes = lax.dynamic_slice_in_dim(routes, position * own_rows, own_rows, 0)
+    own_slots = slot_table(own_routes, experts, capacity, here)
+    place_ids = lax.broadcasted_iota(jnp.int32, (places,) + own_slots.shape, 0)
+    one_hot = jnp.sum((place_ids == own_slots[None]).astype(jnp.float32), axis=2).astype(
+        jnp.bfloat16
+    )
+    chosen = (
+        lax.broadcasted_iota(jnp.int32, (own_rows, top_count, places), 2) == own_slots[:, :, None]
+    )
+    mixing = jnp.sum(jnp.where(chosen, chosen_expert_weight[:, :, None], 0.0), axis=1)
+    mixing_high = mixing.astype(jnp.bfloat16)
+    mixing_low = (mixing - mixing_high.astype(jnp.float32)).astype(jnp.bfloat16)
+
     heads_out = mix_tokens(
         value_projected,
         key_projected,
@@ -237,12 +328,7 @@
         query_filter_weight,
         head_norm_gain,
     )
-    projected = jnp.dot(
-        lax.all_gather(heads_out, "tp", axis=1, tiled=True),
-        mixer_output_matrix,
-        preferred_element_type=jnp.float32,
-    ).astype(jnp.bfloat16)
-    mixer_out = lax.all_to_all(projected, "tp", split_axis=0, concat_axis=1, tiled=True)
+    mixer_out = reduce_columns(heads_out, own_columns, mixer_output_matrix.shape[1])
     middle = (residual_layer_input.astype(jnp.float32) + mixer_out.astype(jnp.float32)).astype(
         jnp.bfloat16
     )
@@ -252,46 +338,27 @@
         * lax.rsqrt(jnp.mean(residual * residual, axis=-1, keepdims=True) + epsilon)
         * expert_norm_gain
     ).astype(jnp.bfloat16)
-    own_rows = normed.shape[0]
-    model_width = normed.shape[1]
-    top_count = routes.shape[1]
-    experts = lax.axis_size("sp")
-    capacity = 2 * own_rows * top_count // experts
-    places = experts * capacity
-    position = lax.axis_index("tp")
-    own_routes = lax.dynamic_slice_in_dim(routes, position * own_rows, own_rows, 0)
-    own_slots = slot_table(own_routes, experts, capacity)
-    outgoing = dispatch_rows(own_slots, normed, places)
-    received = lax.all_to_all(
-        outgoing.reshape(experts, capacity, model_width),
-        "sp",
-        split_axis=0,
-        concat_axis=0,
-        tiled=True,
-    )
-    arrived = lax.all_gather(received[None], "tp", axis=0, tiled=True)
-    slot_rows = arrived.reshape(-1, model_width)
-    gate_value = jnp.dot(slot_rows, expert_gate_matrix[0], preferred_element_type=jnp.float32)
-    up_value = jnp.dot(slot_rows, expert_up_matrix[0], preferred_element_type=jnp.float32)
-    hidden = (jax.nn.silu(gate_value) * up_value).astype(jnp.bfloat16)
-    partial_sum = jnp.dot(hidden, expert_down_matrix[0], preferred_element_type=jnp.float32).astype(
-        jnp.bfloat16
-    )
-    summed = lax.psum_scatter(
-        partial_sum.astype(jnp.float32).reshape(arrived.shape).astype(jnp.bfloat16),
-        "tp",
-        scatter_dimension=0,
-        tiled=True,
-    )
-    results = summed.reshape(experts, capacity, model_width)
-    returned = lax.all_to_all(results, "sp", split_axis=0, concat_axis=0, tiled=True)
-    chosen = (
-        lax.broadcasted_iota(jnp.int32, (own_rows, top_count, places), 2) == own_slots[:, :, None]
-    )
-    mixing = jnp.sum(jnp.where(chosen, chosen_expert_weight[:, :, None], 0.0), axis=1)
-    expert_mix = jnp.dot(
-        mixing, returned.reshape(places, model_width).astype(jnp.float32), precision=highest
-    )
+    outgoing = jnp.dot(one_hot, normed, preferred_element_type=jnp.float32).astype(jnp.bfloat16)
+    outgoing = outgoing.reshape(experts, capacity, model_width)
+    returned = []
+    for chunk in chunks_of(experts):
+        arrived = [exchange(outgoing[d], "sp", d) if d else outgoing[d] for d in chunk]
+        blocks, _ = gather_rows(jnp.concatenate(arrived, axis=0), "tp")
+        slot_rows = blocks.reshape(-1, model_width)
+        gate_value = jnp.dot(slot_rows, expert_gate_matrix[0], preferred_element_type=jnp.float32)
+        up_value = jnp.dot(slot_rows, expert_up_matrix[0], preferred_element_type=jnp.float32)
+        hidden = (jax.nn.silu(gate_value) * up_value).astype(jnp.bfloat16)
+        partial_sum = jnp.dot(
+            hidden, expert_down_matrix[0], preferred_element_type=jnp.float32
+        ).astype(jnp.bfloat16)
+        summed = scatter_rows(partial_sum.reshape(blocks.shape), "tp")
+        results = summed.reshape(len(chunk), capacity, model_width)
+        returned += [
+            exchange(results[i], "sp", d) if d else results[i] for i, d in enumerate(chunk)
+        ]
+    returned = jnp.concatenate(returned, axis=0)
+    expert_mix = jnp.dot(mixing_high, returned, preferred_element_type=jnp.float32)
+    expert_mix = expert_mix + jnp.dot(mixing_low, returned, preferred_element_type=jnp.float32)
     return (residual + expert_mix).astype(jnp.bfloat16)
 
 

time: 368 us -> 261 us (0.71)
  waiting for transfers between devices: 183 us -> 81.7 us
  blocking collectives: 68.4 us -> 0 us
  starting transfers between devices: 15.6 us -> 62.9 us
  local copies, waits for them, and re-layouts: 18.2 us -> 37.3 us
  matrix products: 36.4 us -> 50.9 us
  between operations: 13.9 us -> 1.25 us
  other arithmetic: 31.6 us -> 25.6 us
    all_gather x4 -> x0, waiting for transfers between devices: 85.8 us -> none  [the longest x1 32.8 us: shards(): arrived = lax.all_gather(received[None], 'tp', axis=0, tiled=True)]
    ppermute x0 -> x31, waiting for transfers between devices: none -> 48.1 us  [exchange(): return lax.ppermute(x, axis, [(i, i ^ distance) for i in range(count)])]
    ppermute x0 -> x31, starting transfers between devices: none -> 46.3 us  [exchange(): return lax.ppermute(x, axis, [(i, i ^ distance) for i in range(count)])]
    reduce_scatter x1 -> x0, waiting for transfers between devices: 44.7 us -> none  [shards(): lax.psum_scatter(partial_sum.astype(jnp.float32).reshape(arrived.shape).a...]
    all_gather x2 -> x0, blocking collectives: 37.5 us -> none  [carried_in(): lax.all_gather(part.astype(kind), axis)]
    all_to_all x1 -> x0, blocking collectives: 30.9 us -> none  [shards(): lax.all_to_all(outgoing.reshape(experts, capacity, model_width), 'sp', sp...]
    dot_general x1 -> x3, matrix products: 6.06 us -> 25.2 us  [shards(): jnp.dot(hidden, expert_down_matrix[0], preferred_element_type=jnp.float32)]
    all_to_all x2, waiting for transfers between devices: 31.3 us -> 13.4 us  [the longest x1 9.05 us: carried_states(): back = lax.all_to_all(answer, 'sp', split_axis=0, concat_axis=0, tiled=True)]
  transfers between devices with their start and end apart: 9 -> 35, of which waited for: 7 -> 16; matrix products, arithmetic and copies ran while one was open for 9% -> 32% of each run, Pallas kernels for 0% -> 0%
where the time goes in v1:
time: 261 us; the launch traced here: 260 us
  waiting for transfers between devices  81.7 us (31%)
  starting transfers between devices  62.9 us (24%)
  matrix products  50.9 us (20%)
  local copies, waits for them, and re-layouts  37.3 us (14%)
  other arithmetic  25.6 us (10%)
    ppermute x31, waiting for transfers between devices, exchange(): return lax.ppermute(x, axis, [(i, i ^ distance) for i in range(count)])  48.1 us
    ppermute x31, starting transfers between devices, exchange(): return lax.ppermute(x, axis, [(i, i ^ distance) for i in range(count)])  46.3 us
    dot_general x3, matrix products, shards(): jnp.dot(hidden, expert_down_matrix[0], preferred_element_type=jnp.float32)  25.2 us
    ppermute x1, waiting for transfers between devices, padded_2(): lax.ppermute(tail, axis, [(i, (i + 1) % count) for i in range(ends)])  20.2 us
    unnamed x73, local copies, waits for them, and re-layouts  9.3 us
    all_to_all x1, waiting for transfers between devices, carried_states(): back = lax.all_to_all(answer, 'sp', split_axis=0, concat_axis=0, tiled=True)  9.05 us
    dot_general x3, matrix products, shards(): jnp.dot(slot_rows, expert_up_matrix[0], preferred_element_type=jnp.float32)  8.28 us
    slice x6, local copies, waits for them, and re-layouts, scatter_rows(): received = exchange(blocks[half:], axis, bit)  7.12 us
  transfers between devices with their start and end apart: 35, of which 16 were waited for; matrix products, arithmetic and copies ran while one was open for 32% of the time, Pallas kernels for 0%

profile of v1, /device:TPU:0, one launch (start us, length us, event | category | flops | bytes accessed | tf_op | source)
XLA Modules:
  0.0 259.7 jit_solution(15553405290631940020)
XLA Ops:
  4.8 4.9 %collective-permute-start = (bf16[2,2048]{0,1:T(8,128)(2,1)}, bf16[2,2048]{0,1:T(8,128)(2,1)S(1)}, u32[]{:S(2)}, u32[]{:S(2)}) collective-permute-start(bf16[2,2048]{0,1:T(8,128)(2,1)} %get-tuple-element.245), channel_id=1, source_target_pairs={{0,4},{4,8},{8,12},{12,16},{16,20},{20,24},{24,28},{1,5},{5,9},{9,... | collective-permute-start | bytes 24584 | tf_op jit(solution)/shard_map/ppermute | solution.py:24
  12.2 20.2 %collective-permute-done = bf16[2,2048]{0,1:T(8,128)(2,1)S(1)} collective-permute-done((bf16[2,2048]{0,1:T(8,128)(2,1)}, bf16[2,2048]{0,1:T(8,128)(2,1)S(1)}, u32[]{:S(2)}, u32[]{:S(2)}) %collective-permute-start) | collective-permute-done | bytes 8224 | tf_op jit(solution)/shard_map/ppermute | solution.py:24
  33.2 3.9 %fusion.29 = f32[256,2048]{0,1:T(8,128)S(1)} fusion(f32[260,2048]{0,1:T(8,128)S(1)} %maximum_convert_fusion, f32[2048]{0:T(1024)S(1)} %bitcast.400, f32[2048]{0:T(1024)S(1)} %bitcast.397, f32[2048]{0:T(1024)S(1)} %bitcast.398, f32[2048]{0:T(1024)S(1)} %bitcast.399, f32[2048]{0:T(1024)S(1)} %bitcast.396), kind=kLoop, calls=%fused_computation.32 | loop fusion | flops 4718592 | bytes 12623872 | tf_op jit(solution)/shard_map/add | solution.py:109
  49.2 6.7 %all-to-all-start = ((bf16[8,16,2112]{2,1,0:T(8,128)(2,1)}), bf16[8,16,2112]{2,1,0:T(8,128)(2,1)}, u32[]{:S(2)}, u32[]{:S(2)}) async-start(bf16[8,16,2112]{2,1,0:T(8,128)(2,1)} %bitcast.18), calls=%async_computation | async-start | bytes 1114112 | tf_op jit(solution)/shard_map/all_to_all | solution.py:45
  55.9 3.7 %constant_dynamic-slice_fusion.4 = (bf16[1024,512]{1,0:T(8,128)(2,1)}, bf16[1024,512]{1,0:T(8,128)(2,1)}, bf16[1024,512]{1,0:T(8,128)(2,1)}) fusion(bf16[4096,512]{1,0:T(8,128)(2,1)} %param.35, s32[]{:T(128)S(6)} %select_n.95, s32[]{:T(128)S(6)} %select_n.97, s32[]{:T(128)S(6)} %select_n.96), kind=kLoop, calls=%fused_computation.267 | loop fusion | bytes 6291468 | tf_op jit(solution)/shard_map/dynamic_slice | solution.py:266
  62.6 2.6 reshape.391
  67.0 4.3 %all-to-all-done = bf16[8,16,2112]{2,1,0:T(8,128)(2,1)} async-done(((bf16[8,16,2112]{2,1,0:T(8,128)(2,1)}), bf16[8,16,2112]{2,1,0:T(8,128)(2,1)}, u32[]{:S(2)}, u32[]{:S(2)}) %all-to-all-start) | async-done | bytes 540704 | tf_op jit(solution)/shard_map/all_to_all | solution.py:45
  78.7 3.8 %all-to-all-start.1 = ((bf16[8,16,2048]{2,1,0:T(8,128)(2,1)}), bf16[8,16,2048]{2,1,0:T(8,128)(2,1)S(1)}, u32[]{:S(2)}, u32[]{:S(2)}) async-start(bf16[8,16,2048]{2,1,0:T(8,128)(2,1)} %bitcast_dynamic-update-slice_fusion.2), calls=%async_computation.1 | async-start | bytes 1048576 | tf_op jit(solution)/shard_map/all_to_all | solution.py:61
  88.1 9.0 %all-to-all-done.1 = bf16[8,16,2048]{2,1,0:T(8,128)(2,1)S(1)} async-done(((bf16[8,16,2048]{2,1,0:T(8,128)(2,1)}), bf16[8,16,2048]{2,1,0:T(8,128)(2,1)S(1)}, u32[]{:S(2)}, u32[]{:S(2)}) %all-to-all-start.1) | async-done | bytes 524320 | tf_op jit(solution)/shard_map/all_to_all | solution.py:61
  115.9 6.7 %collective-permute-done.6 = bf16[1,64,4,512]{3,1,0,2:T(8,128)(2,1)S(1)} collective-permute-done((bf16[1,64,4,512]{3,1,0,2:T(8,128)(2,1)S(1)}, bf16[1,64,4,512]{3,1,0,2:T(8,128)(2,1)S(1)}, u32[]{:S(2)}, u32[]{:S(2)}) %collective-permute-start.6) | collective-permute-done | bytes 262176 | tf_op jit(solution)/shard_map/ppermute | solution.py:198
  126.1 3.4 %collective-permute-start.26 = (bf16[32,2048]{1,0:T(8,128)(2,1)S(1)}, bf16[32,2048]{1,0:T(8,128)(2,1)S(1)}, u32[]{:S(2)}, u32[]{:S(2)}) collective-permute-start(bf16[32,2048]{1,0:T(8,128)(2,1)S(1)} %get-tuple-element.232), channel_id=1, source_target_pairs={{0,28},{4,24},{8,20},{12,16},{16,12},{20,8},{24,4},{28,0},{1,29},{... | collective-permute-start | bytes 393224 | tf_op jit(solution)/shard_map/ppermute | solution.py:198
  129.6 2.9 %collective-permute-start.18 = (bf16[32,2048]{1,0:T(8,128)(2,1)S(1)}, bf16[32,2048]{1,0:T(8,128)(2,1)S(1)}, u32[]{:S(2)}, u32[]{:S(2)}) collective-permute-start(bf16[32,2048]{1,0:T(8,128)(2,1)S(1)} %get-tuple-element.233), channel_id=1, source_target_pairs={{0,20},{4,16},{8,28},{12,24},{16,4},{20,0},{24,12},{28,8},{1,21},{... | collective-permute-start | bytes 393224 | tf_op jit(solution)/shard_map/ppermute | solution.py:198
  133.9 9.2 %collective-permute-start.8 = (bf16[32,2048]{1,0:T(8,128)(2,1)S(1)}, bf16[32,2048]{1,0:T(8,128)(2,1)S(1)}, u32[]{:S(2)}, u32[]{:S(2)}) collective-permute-start(bf16[32,2048]{1,0:T(8,128)(2,1)S(1)} %get-tuple-element.236), channel_id=1, source_target_pairs={{0,8},{4,12},{8,0},{12,4},{16,24},{20,28},{24,16},{28,20},{1,9},{5... | collective-permute-start | bytes 393224 | tf_op jit(solution)/shard_map/ppermute | solution.py:198
  143.2 3.7 %collective-permute-start.9 = (bf16[32,2048]{1,0:T(8,128)(2,1)S(1)}, bf16[32,2048]{1,0:T(8,128)(2,1)S(1)}, u32[]{:S(2)}, u32[]{:S(2)}) collective-permute-start(bf16[32,2048]{1,0:T(8,128)(2,1)S(1)} %get-tuple-element.235), channel_id=1, source_target_pairs={{0,12},{4,8},{8,4},{12,0},{16,28},{20,24},{24,20},{28,16},{1,13},{... | collective-permute-start | bytes 393224 | tf_op jit(solution)/shard_map/ppermute | solution.py:198
  154.5 2.7 %collective-permute-done.27 = bf16[1,64,2048]{2,1,0:T(8,128)(2,1)S(1)} collective-permute-done((bf16[1,64,2048]{2,1,0:T(8,128)(2,1)S(1)}, bf16[1,64,2048]{2,1,0:T(8,128)(2,1)S(1)}, u32[]{:S(2)}, u32[]{:S(2)}) %collective-permute-start.27) | collective-permute-done | bytes 262176 | tf_op jit(solution)/shard_map/ppermute | solution.py:198
  157.5 5.4 %collective-permute-done.19 = bf16[1,64,2048]{2,1,0:T(8,128)(2,1)S(1)} collective-permute-done((bf16[1,64,2048]{2,1,0:T(8,128)(2,1)S(1)}, bf16[1,64,2048]{2,1,0:T(8,128)(2,1)S(1)}, u32[]{:S(2)}, u32[]{:S(2)}) %collective-permute-start.19) | collective-permute-done | bytes 262176 | tf_op jit(solution)/shard_map/ppermute | solution.py:198
  163.7 6.1 %collective-permute-done.10 = bf16[1,128,2048]{2,1,0:T(8,128)(2,1)S(1)} collective-permute-done((bf16[1,128,2048]{2,1,0:T(8,128)(2,1)S(1)}, bf16[1,128,2048]{2,1,0:T(8,128)(2,1)S(1)}, u32[]{:S(2)}, u32[]{:S(2)}) %collective-permute-start.10) | collective-permute-done | bytes 524320 | tf_op jit(solution)/shard_map/ppermute | solution.py:198
  172.0 2.3 fusion.6
  174.2 7.4 %fusion.24 = bf16[256,2048]{1,0:T(8,128)(2,1)} fusion(bf16[1,1024,2048]{2,1,0:T(8,128)(2,1)} %param.41, f32[256,1024]{1,0:T(8,128)} %fusion.6, bf16[256,2048]{1,0:T(8,128)(2,1)} %bitcast.375, bf16[1,2048,1024]{2,1,0:T(8,128)(2,1)} %param.39), kind=kOutput, calls=%fused_computation.26 | convolution fusion | flops 2149580800 | bytes 11534336 | tf_op jit(solution)/shard_map/dot_general | solution.py:351
  186.5 2.3 fusion.8
  188.8 7.7 %fusion.21 = bf16[256,2048]{1,0:T(8,128)(2,1)} fusion(bf16[1,1024,2048]{2,1,0:T(8,128)(2,1)} %param.41, f32[256,1024]{1,0:T(8,128)} %fusion.8, bf16[256,2048]{1,0:T(8,128)(2,1)} %bitcast.377, bf16[1,2048,1024]{2,1,0:T(8,128)(2,1)} %param.39), kind=kOutput, calls=%fused_computation.25 | convolution fusion | flops 2149580800 | bytes 11534336 | tf_op jit(solution)/shard_map/dot_general | solution.py:351
  196.5 2.4 fusion.158
  202.7 3.7 %fusion.10 = f32[512,1024]{1,0:T(8,128)} fusion(bf16[512,2048]{1,0:T(8,128)(2,1)S(1)} %bitcast.369, bf16[1,2048,1024]{2,1,0:T(8,128)(2,1)S(1)} %copy-done.29), kind=kOutput, calls=%fused_computation.16 | convolution fusion | flops 2147483648 | bytes 8388608 | tf_op jit(solution)/shard_map/dot_general | solution.py:349
  206.4 10.1 %fusion.18 = bf16[512,2048]{1,0:T(8,128)(2,1)} fusion(bf16[1,1024,2048]{2,1,0:T(8,128)(2,1)} %param.41, f32[512,1024]{1,0:T(8,128)} %fusion.10, bf16[512,2048]{1,0:T(8,128)(2,1)S(1)} %bitcast.370, bf16[1,2048,1024]{2,1,0:T(8,128)(2,1)} %param.39), kind=kOutput, calls=%fused_computation.24 | convolution fusion | flops 4299161600 | bytes 14680064 | tf_op jit(solution)/shard_map/dot_general | solution.py:351
  222.2 2.5 collective-permute-start.31
  225.9 3.1 %collective-permute-done.22 = bf16[1,64,2048]{2,1,0:T(8,128)(2,1)S(1)} collective-permute-done((bf16[1,64,2048]{2,1,0:T(8,128)(2,1)S(1)}, bf16[1,64,2048]{2,1,0:T(8,128)(2,1)S(1)}, u32[]{:S(2)}, u32[]{:S(2)}) %collective-permute-start.22) | collective-permute-done | bytes 262176 | tf_op jit(solution)/shard_map/ppermute | solution.py:198
  229.2 3.9 %collective-permute-start.24 = (bf16[32,2048]{1,0:T(8,128)(2,1)S(1)}, bf16[32,2048]{1,0:T(8,128)(2,1)S(1)}, u32[]{:S(2)}, u32[]{:S(2)}) collective-permute-start(bf16[32,2048]{1,0:T(8,128)(2,1)S(1)} %get-tuple-element.256), channel_id=1, source_target_pairs={{0,20},{4,16},{8,28},{12,24},{16,4},{20,0},{24,12},{28,8},{1,21},{... | collective-permute-start | bytes 393224 | tf_op jit(solution)/shard_map/ppermute | solution.py:198
  233.1 2.3 collective-permute-start.32
  235.4 4.2 %collective-permute-done.13 = bf16[1,128,2048]{2,1,0:T(8,128)(2,1)S(1)} collective-permute-done((bf16[1,128,2048]{2,1,0:T(8,128)(2,1)S(1)}, bf16[1,128,2048]{2,1,0:T(8,128)(2,1)S(1)}, u32[]{:S(2)}, u32[]{:S(2)}) %collective-permute-start.13) | collective-permute-done | bytes 524320 | tf_op jit(solution)/shard_map/ppermute | solution.py:198
  241.4 6.0 %collective-permute-done.14 = bf16[32,2048]{1,0:T(8,128)(2,1)S(1)} collective-permute-done((bf16[32,2048]{1,0:T(8,128)(2,1)S(1)}, bf16[32,2048]{1,0:T(8,128)(2,1)S(1)}, u32[]{:S(2)}, u32[]{:S(2)}) %collective-permute-start.14) | collective-permute-done | bytes 131104 | tf_op jit(solution)/shard_map/ppermute | solution.py:198
  247.4 5.0 %collective-permute-done.15 = bf16[32,2048]{1,0:T(8,128)(2,1)S(1)} collective-permute-done((bf16[32,2048]{1,0:T(8,128)(2,1)S(1)}, bf16[32,2048]{1,0:T(8,128)(2,1)S(1)}, u32[]{:S(2)}, u32[]{:S(2)}) %collective-permute-start.15) | collective-permute-done | bytes 131104 | tf_op jit(solution)/shard_map/ppermute | solution.py:198
  253.7 4.6 %collective-permute-done.16 = bf16[32,2048]{1,0:T(8,128)(2,1)S(1)} collective-permute-done((bf16[32,2048]{1,0:T(8,128)(2,1)S(1)}, bf16[32,2048]{1,0:T(8,128)(2,1)S(1)}, u32[]{:S(2)}, u32[]{:S(2)}) %collective-permute-start.16) | collective-permute-done | bytes 131104 | tf_op jit(solution)/shard_map/ppermute | solution.py:198
  (276 shorter events, 94.1 us)
Async XLA Ops:
  4.8 27.6 %collective-permute-start = (bf16[2,2048]{0,1:T(8,128)(2,1)}, bf16[2,2048]{0,1:T(8,128)(2,1)S(1)}, u32[]{:S(2)}, u32[]{:S(2)}) collective-permute-start(bf16[2,2048]{0,1:T(8,128)(2,1)} %get-tuple-element.245), channel_id=1, source_target_pairs={{0,4},{4,8},{8,12},{12,16},{16,20},{20,24},{24,28},{1,5},{5,9},{9,... | collective-permute-start | bytes 24584 | tf_op jit(solution)/shard_map/ppermute | solution.py:24
  9.7 22.7 %collective-permute-start.1 = (bf16[2,2048]{0,1:T(8,128)(2,1)}, bf16[2,2048]{0,1:T(8,128)(2,1)S(1)}, u32[]{:S(2)}, u32[]{:S(2)}) collective-permute-start(bf16[2,2048]{0,1:T(8,128)(2,1)} %get-tuple-element.246), channel_id=1, source_target_pairs={{4,0},{8,4},{12,8},{16,12},{20,16},{24,20},{28,24},{5,1},{9,5},{13... | collective-permute-start | bytes 24584 | tf_op jit(solution)/shard_map/ppermute | solution.py:26
  49.2 22.1 %all-to-all-start = ((bf16[8,16,2112]{2,1,0:T(8,128)(2,1)}), bf16[8,16,2112]{2,1,0:T(8,128)(2,1)}, u32[]{:S(2)}, u32[]{:S(2)}) async-start(bf16[8,16,2112]{2,1,0:T(8,128)(2,1)} %bitcast.18), calls=%async_computation | async-start | bytes 1114112 | tf_op jit(solution)/shard_map/all_to_all | solution.py:45
  59.5 47.2 %collective-permute-start.2 = (bf16[1024,512]{1,0:T(8,128)(2,1)}, bf16[1024,512]{1,0:T(8,128)(2,1)}, u32[]{:S(2)}, u32[]{:S(2)}) collective-permute-start(bf16[1024,512]{1,0:T(8,128)(2,1)} %get-tuple-element.215), channel_id=1, source_target_pairs={{0,1},{1,0},{2,3},{3,2},{4,5},{5,4},{6,7},{7,6},{8,9},{9,8},{10,11... | collective-permute-start | bytes 3145736 | tf_op jit(solution)/shard_map/ppermute | solution.py:198
  59.5 48.9 %collective-permute-start.3 = (bf16[1024,512]{1,0:T(8,128)(2,1)}, bf16[1024,512]{1,0:T(8,128)(2,1)}, u32[]{:S(2)}, u32[]{:S(2)}) collective-permute-start(bf16[1024,512]{1,0:T(8,128)(2,1)} %get-tuple-element.217), channel_id=1, source_target_pairs={{0,2},{1,3},{2,0},{3,1},{4,6},{5,7},{6,4},{7,5},{8,10},{9,11},{10,... | collective-permute-start | bytes 3145736 | tf_op jit(solution)/shard_map/ppermute | solution.py:198
  61.0 49.1 %collective-permute-start.4 = (bf16[1024,512]{1,0:T(8,128)(2,1)}, bf16[1024,512]{1,0:T(8,128)(2,1)}, u32[]{:S(2)}, u32[]{:S(2)}) collective-permute-start(bf16[1024,512]{1,0:T(8,128)(2,1)} %get-tuple-element.216), channel_id=1, source_target_pairs={{0,3},{1,2},{2,1},{3,0},{4,7},{5,6},{6,5},{7,4},{8,11},{9,10},{10,... | collective-permute-start | bytes 3145736 | tf_op jit(solution)/shard_map/ppermute | solution.py:198
  78.7 18.4 %all-to-all-start.1 = ((bf16[8,16,2048]{2,1,0:T(8,128)(2,1)}), bf16[8,16,2048]{2,1,0:T(8,128)(2,1)S(1)}, u32[]{:S(2)}, u32[]{:S(2)}) async-start(bf16[8,16,2048]{2,1,0:T(8,128)(2,1)} %bitcast_dynamic-update-slice_fusion.2), calls=%async_computation.1 | async-start | bytes 1048576 | tf_op jit(solution)/shard_map/all_to_all | solution.py:61
  114.2 8.4 %collective-permute-start.6 = (bf16[1,64,4,512]{3,1,0,2:T(8,128)(2,1)S(1)}, bf16[1,64,4,512]{3,1,0,2:T(8,128)(2,1)S(1)}, u32[]{:S(2)}, u32[]{:S(2)}) collective-permute-start(bf16[1,64,4,512]{3,1,0,2:T(8,128)(2,1)S(1)} %constant_dynamic-slice_fusion.1), channel_id=1, source_target_pairs={{0,2},{1,3},{2,0},{3,1},{4,6},{5,7},{6,4},{7,5},{8,10},{9,11},{10,... | collective-permute-start | bytes 786440 | tf_op jit(solution)/shard_map/ppermute | solution.py:198
  124.8 9.2 %collective-permute-start.25 = (bf16[32,2048]{1,0:T(8,128)(2,1)S(1)}, bf16[32,2048]{1,0:T(8,128)(2,1)S(1)}, u32[]{:S(2)}, u32[]{:S(2)}) collective-permute-start(bf16[32,2048]{1,0:T(8,128)(2,1)S(1)} %get-tuple-element.231), channel_id=1, source_target_pairs={{0,24},{4,28},{8,16},{12,20},{16,8},{20,12},{24,0},{28,4},{1,25},{... | collective-permute-start | bytes 393224 | tf_op jit(solution)/shard_map/ppermute | solution.py:198
  126.1 17.1 %collective-permute-start.26 = (bf16[32,2048]{1,0:T(8,128)(2,1)S(1)}, bf16[32,2048]{1,0:T(8,128)(2,1)S(1)}, u32[]{:S(2)}, u32[]{:S(2)}) collective-permute-start(bf16[32,2048]{1,0:T(8,128)(2,1)S(1)} %get-tuple-element.232), channel_id=1, source_target_pairs={{0,28},{4,24},{8,20},{12,16},{16,12},{20,8},{24,4},{28,0},{1,29},{... | collective-permute-start | bytes 393224 | tf_op jit(solution)/shard_map/ppermute | solution.py:198
  129.5 18.5 %collective-permute-start.17 = (bf16[32,2048]{1,0:T(8,128)(2,1)S(1)}, bf16[32,2048]{1,0:T(8,128)(2,1)S(1)}, u32[]{:S(2)}, u32[]{:S(2)}) collective-permute-start(bf16[32,2048]{1,0:T(8,128)(2,1)S(1)} %get-tuple-element.234), channel_id=1, source_target_pairs={{0,16},{4,20},{8,24},{12,28},{16,0},{20,4},{24,8},{28,12},{1,17},{... | collective-permute-start | bytes 393224 | tf_op jit(solution)/shard_map/ppermute | solution.py:198
  129.6 20.0 %collective-permute-start.18 = (bf16[32,2048]{1,0:T(8,128)(2,1)S(1)}, bf16[32,2048]{1,0:T(8,128)(2,1)S(1)}, u32[]{:S(2)}, u32[]{:S(2)}) collective-permute-start(bf16[32,2048]{1,0:T(8,128)(2,1)S(1)} %get-tuple-element.233), channel_id=1, source_target_pairs={{0,20},{4,16},{8,28},{12,24},{16,4},{20,0},{24,12},{28,8},{1,21},{... | collective-permute-start | bytes 393224 | tf_op jit(solution)/shard_map/ppermute | solution.py:198
  132.5 18.4 %collective-permute-start.7 = (bf16[32,2048]{1,0:T(8,128)(2,1)S(1)}, bf16[32,2048]{1,0:T(8,128)(2,1)S(1)}, u32[]{:S(2)}, u32[]{:S(2)}) collective-permute-start(bf16[32,2048]{1,0:T(8,128)(2,1)S(1)} %get-tuple-element.237), channel_id=1, source_target_pairs={{0,4},{4,0},{8,12},{12,8},{16,20},{20,16},{24,28},{28,24},{1,5},{5... | collective-permute-start | bytes 393224 | tf_op jit(solution)/shard_map/ppermute | solution.py:198
  133.9 17.1 %collective-permute-start.8 = (bf16[32,2048]{1,0:T(8,128)(2,1)S(1)}, bf16[32,2048]{1,0:T(8,128)(2,1)S(1)}, u32[]{:S(2)}, u32[]{:S(2)}) collective-permute-start(bf16[32,2048]{1,0:T(8,128)(2,1)S(1)} %get-tuple-element.236), channel_id=1, source_target_pairs={{0,8},{4,12},{8,0},{12,4},{16,24},{20,28},{24,16},{28,20},{1,9},{5... | collective-permute-start | bytes 393224 | tf_op jit(solution)/shard_map/ppermute | solution.py:198
  143.2 9.7 %collective-permute-start.9 = (bf16[32,2048]{1,0:T(8,128)(2,1)S(1)}, bf16[32,2048]{1,0:T(8,128)(2,1)S(1)}, u32[]{:S(2)}, u32[]{:S(2)}) collective-permute-start(bf16[32,2048]{1,0:T(8,128)(2,1)S(1)} %get-tuple-element.235), channel_id=1, source_target_pairs={{0,12},{4,8},{8,4},{12,0},{16,28},{20,24},{24,20},{28,16},{1,13},{... | collective-permute-start | bytes 393224 | tf_op jit(solution)/shard_map/ppermute | solution.py:198
  148.1 9.2 %collective-permute-start.27 = (bf16[1,64,2048]{2,1,0:T(8,128)(2,1)S(1)}, bf16[1,64,2048]{2,1,0:T(8,128)(2,1)S(1)}, u32[]{:S(2)}, u32[]{:S(2)}) collective-permute-start(bf16[1,64,2048]{2,1,0:T(8,128)(2,1)S(1)} %maximum_bitcast_fusion.3), channel_id=1, source_target_pairs={{0,2},{1,3},{2,0},{3,1},{4,6},{5,7},{6,4},{7,5},{8,10},{9,11},{10,... | collective-permute-start | bytes 786440 | tf_op jit(solution)/shard_map/ppermute | solution.py:198
  149.6 13.2 %collective-permute-start.19 = (bf16[1,64,2048]{2,1,0:T(8,128)(2,1)S(1)}, bf16[1,64,2048]{2,1,0:T(8,128)(2,1)S(1)}, u32[]{:S(2)}, u32[]{:S(2)}) collective-permute-start(bf16[1,64,2048]{2,1,0:T(8,128)(2,1)S(1)} %maximum_bitcast_fusion.2), channel_id=1, source_target_pairs={{0,2},{1,3},{2,0},{3,1},{4,6},{5,7},{6,4},{7,5},{8,10},{9,11},{10,... | collective-permute-start | bytes 786440 | tf_op jit(solution)/shard_map/ppermute | solution.py:198
  153.0 16.9 %collective-permute-start.10 = (bf16[1,128,2048]{2,1,0:T(8,128)(2,1)S(1)}, bf16[1,128,2048]{2,1,0:T(8,128)(2,1)S(1)}, u32[]{:S(2)}, u32[]{:S(2)}) collective-permute-start(bf16[1,128,2048]{2,1,0:T(8,128)(2,1)S(1)} %maximum_bitcast_fusion), channel_id=1, source_target_pairs={{0,2},{1,3},{2,0},{3,1},{4,6},{5,7},{6,4},{7,5},{8,10},{9,11},{10,... | collective-permute-start | bytes 1572872 | tf_op jit(solution)/shard_map/ppermute | solution.py:198
  157.3 13.5 %collective-permute-start.28 = (bf16[2,64,2048]{2,1,0:T(8,128)(2,1)S(1)}, bf16[2,64,2048]{2,1,0:T(8,128)(2,1)S(1)}, u32[]{:S(2)}, u32[]{:S(2)}) collective-permute-start(bf16[2,64,2048]{2,1,0:T(8,128)(2,1)S(1)} %pad_maximum_fusion.7), channel_id=1, source_target_pairs={{0,1},{1,0},{2,3},{3,2},{4,5},{5,4},{6,7},{7,6},{8,9},{9,8},{10,11... | collective-permute-start | bytes 1572872 | tf_op jit(solution)/shard_map/ppermute | solution.py:198
  163.7 20.7 %collective-permute-start.20 = (bf16[2,64,2048]{2,1,0:T(8,128)(2,1)}, bf16[2,64,2048]{2,1,0:T(8,128)(2,1)}, u32[]{:S(2)}, u32[]{:S(2)}) collective-permute-start(bf16[2,64,2048]{2,1,0:T(8,128)(2,1)} %pad_maximum_fusion.6), channel_id=1, source_target_pairs={{0,1},{1,0},{2,3},{3,2},{4,5},{5,4},{6,7},{7,6},{8,9},{9,8},{10,11... | collective-permute-start | bytes 1572872 | tf_op jit(solution)/shard_map/ppermute | solution.py:198
  170.7 30.5 %collective-permute-start.11 = (bf16[2,128,2048]{2,1,0:T(8,128)(2,1)S(1)}, bf16[2,128,2048]{2,1,0:T(8,128)(2,1)}, u32[]{:S(2)}, u32[]{:S(2)}) collective-permute-start(bf16[2,128,2048]{2,1,0:T(8,128)(2,1)S(1)} %pad_maximum_fusion.3), channel_id=1, source_target_pairs={{0,1},{1,0},{2,3},{3,2},{4,5},{5,4},{6,7},{7,6},{8,9},{9,8},{10,11... | collective-permute-start | bytes 3145736 | tf_op jit(solution)/shard_map/ppermute | solution.py:198
  183.9 14.9 %collective-permute-start.29 = (bf16[2,64,2048]{2,1,0:T(8,128)(2,1)}, bf16[2,64,2048]{2,1,0:T(8,128)(2,1)S(1)}, u32[]{:S(2)}, u32[]{:S(2)}) collective-permute-start(bf16[2,64,2048]{2,1,0:T(8,128)(2,1)} %bitcast.94), channel_id=1, source_target_pairs={{0,1},{1,0},{2,3},{3,2},{4,5},{5,4},{6,7},{7,6},{8,9},{9,8},{10,11... | collective-permute-start | bytes 1572872 | tf_op jit(solution)/shard_map/ppermute | solution.py:198
  198.8 19.8 %collective-permute-start.21 = (bf16[2,64,2048]{2,1,0:T(8,128)(2,1)}, bf16[2,64,2048]{2,1,0:T(8,128)(2,1)}, u32[]{:S(2)}, u32[]{:S(2)}) collective-permute-start(bf16[2,64,2048]{2,1,0:T(8,128)(2,1)} %bitcast.88), channel_id=1, source_target_pairs={{0,1},{1,0},{2,3},{3,2},{4,5},{5,4},{6,7},{7,6},{8,9},{9,8},{10,11... | collective-permute-start | bytes 1572872 | tf_op jit(solution)/shard_map/ppermute | solution.py:198
  199.7 21.5 %collective-permute-start.30 = (bf16[1,64,2048]{2,1,0:T(8,128)(2,1)}, bf16[1,64,2048]{2,1,0:T(8,128)(2,1)}, u32[]{:S(2)}, u32[]{:S(2)}) collective-permute-start(bf16[1,64,2048]{2,1,0:T(8,128)(2,1)} %slice.512), channel_id=1, source_target_pairs={{0,2},{1,3},{2,0},{3,1},{4,6},{5,7},{6,4},{7,5},{8,10},{9,11},{10,... | collective-permute-start | bytes 786440 | tf_op jit(solution)/shard_map/ppermute | solution.py:198
  218.3 6.4 %collective-permute-start.12 = (bf16[2,128,2048]{2,1,0:T(8,128)(2,1)S(1)}, bf16[2,128,2048]{2,1,0:T(8,128)(2,1)S(1)}, u32[]{:S(2)}, u32[]{:S(2)}) collective-permute-start(bf16[2,128,2048]{2,1,0:T(8,128)(2,1)S(1)} %bitcast.384), channel_id=1, source_target_pairs={{0,1},{1,0},{2,3},{3,2},{4,5},{5,4},{6,7},{7,6},{8,9},{9,8},{10,11... | collective-permute-start | bytes 3145736 | tf_op jit(solution)/shard_map/ppermute | solution.py:198
  219.8 9.2 %collective-permute-start.22 = (bf16[1,64,2048]{2,1,0:T(8,128)(2,1)S(1)}, bf16[1,64,2048]{2,1,0:T(8,128)(2,1)S(1)}, u32[]{:S(2)}, u32[]{:S(2)}) collective-permute-start(bf16[1,64,2048]{2,1,0:T(8,128)(2,1)S(1)} %slice.504), channel_id=1, source_target_pairs={{0,2},{1,3},{2,0},{3,1},{4,6},{5,7},{6,4},{7,5},{8,10},{9,11},{10,... | collective-permute-start | bytes 786440 | tf_op jit(solution)/shard_map/ppermute | solution.py:198
  222.2 36.1 %collective-permute-start.31 = (bf16[32,2048]{1,0:T(8,128)(2,1)S(1)}, bf16[32,2048]{1,0:T(8,128)(2,1)S(1)}, u32[]{:S(2)}, u32[]{:S(2)}) collective-permute-start(bf16[32,2048]{1,0:T(8,128)(2,1)S(1)} %get-tuple-element.255), channel_id=1, source_target_pairs={{0,24},{4,28},{8,16},{12,20},{16,8},{20,12},{24,0},{28,4},{1,25},{... | collective-permute-start | bytes 393224 | tf_op jit(solution)/shard_map/ppermute | solution.py:198
  225.2 14.4 %collective-permute-start.13 = (bf16[1,128,2048]{2,1,0:T(8,128)(2,1)S(1)}, bf16[1,128,2048]{2,1,0:T(8,128)(2,1)S(1)}, u32[]{:S(2)}, u32[]{:S(2)}) collective-permute-start(bf16[1,128,2048]{2,1,0:T(8,128)(2,1)S(1)} %slice.494), channel_id=1, source_target_pairs={{0,2},{1,3},{2,0},{3,1},{4,6},{5,7},{6,4},{7,5},{8,10},{9,11},{10,... | collective-permute-start | bytes 1572872 | tf_op jit(solution)/shard_map/ppermute | solution.py:198
  229.1 29.1 %collective-permute-start.23 = (bf16[32,2048]{1,0:T(8,128)(2,1)S(1)}, bf16[32,2048]{1,0:T(8,128)(2,1)S(1)}, u32[]{:S(2)}, u32[]{:S(2)}) collective-permute-start(bf16[32,2048]{1,0:T(8,128)(2,1)S(1)} %get-tuple-element.257), channel_id=1, source_target_pairs={{0,16},{4,20},{8,24},{12,28},{16,0},{20,4},{24,8},{28,12},{1,17},{... | collective-permute-start | bytes 393224 | tf_op jit(solution)/shard_map/ppermute | solution.py:198
  229.2 29.1 %collective-permute-start.24 = (bf16[32,2048]{1,0:T(8,128)(2,1)S(1)}, bf16[32,2048]{1,0:T(8,128)(2,1)S(1)}, u32[]{:S(2)}, u32[]{:S(2)}) collective-permute-start(bf16[32,2048]{1,0:T(8,128)(2,1)S(1)} %get-tuple-element.256), channel_id=1, source_target_pairs={{0,20},{4,16},{8,28},{12,24},{16,4},{20,0},{24,12},{28,8},{1,21},{... | collective-permute-start | bytes 393224 | tf_op jit(solution)/shard_map/ppermute | solution.py:198
  233.1 25.2 %collective-permute-start.32 = (bf16[32,2048]{1,0:T(8,128)(2,1)S(1)}, bf16[32,2048]{1,0:T(8,128)(2,1)S(1)}, u32[]{:S(2)}, u32[]{:S(2)}) collective-permute-start(bf16[32,2048]{1,0:T(8,128)(2,1)S(1)} %get-tuple-element.254), channel_id=1, source_target_pairs={{0,28},{4,24},{8,20},{12,16},{16,12},{20,8},{24,4},{28,0},{1,29},{... | collective-permute-start | bytes 393224 | tf_op jit(solution)/shard_map/ppermute | solution.py:198
  239.8 7.6 %collective-permute-start.14 = (bf16[32,2048]{1,0:T(8,128)(2,1)S(1)}, bf16[32,2048]{1,0:T(8,128)(2,1)S(1)}, u32[]{:S(2)}, u32[]{:S(2)}) collective-permute-start(bf16[32,2048]{1,0:T(8,128)(2,1)S(1)} %get-tuple-element.249), channel_id=1, source_target_pairs={{0,4},{4,0},{8,12},{12,8},{16,20},{20,16},{24,28},{28,24},{1,5},{5... | collective-permute-start | bytes 393224 | tf_op jit(solution)/shard_map/ppermute | solution.py:198
  (33 other events, 159.0 us)
